TPU v7x, 32 devices: a whole 2x2x4 slice. The times are simulated.
32 devices in a mesh: fs: 4 (over z), rep: 4 (over y, x), tp: 2 (over core).
Axes of the slice: x: 2, y: 2, z: 4, core: 2. Of those that a mesh axis runs over, the one named last changes fastest.
Arguments:
- saved_input: bfloat16 [16384, 2048], P(('fs', 'rep')), may hold values from -500 to 500
- query_cotangent: bfloat16 [16384, 2048], P(('fs', 'rep'), 'tp'), may hold values from -0.014038086 to 0.014038086
- key_cotangent: bfloat16 [16384, 512], P(('fs', 'rep'), 'tp'), may hold values from -0.014038086 to 0.014038086
- query_weight: float32 [2048, 2048], P('fs', 'tp'), may hold values from -45 to 45
- key_weight: float32 [2048, 512], P('fs', 'tp'), may hold values from -45 to 45
- query_moment: float32 [2048, 2048], P('fs', 'tp'), may hold values from -45 to 45
- key_moment: float32 [2048, 512], P('fs', 'tp'), may hold values from -45 to 45
- query_row_root: bfloat16 [2048, 2048], P('fs'), may hold values from -1 to 3, as said below
- key_row_root: bfloat16 [2048, 2048], P('fs'), may hold values from -1 to 3, as said below
- query_head_root: bfloat16 [32, 64, 64], P('tp'), may hold values from -1 to 3, as said below
- key_head_root: bfloat16 [8, 64, 64], P('tp'), may hold values from -1 to 3, as said below
- query_head_stat: float32 [32, 64, 64], P('tp'), may hold values from -26 to 27, as said below
- key_head_stat: float32 [8, 64, 64], P('tp'), may hold values from -26 to 27, as said below
Outputs:
- query_step: float32 [2048, 2048], P('fs', 'tp')
- key_step: float32 [2048, 512], P('fs', 'tp')
- query_next: float32 [2048, 2048], P('fs', 'tp')
- key_next: float32 [2048, 512], P('fs', 'tp')
- query_copy: bfloat16 [2048, 2048], P(None, 'tp')
- key_copy: bfloat16 [2048, 512], P(None, 'tp')
- query_moment_next: float32 [2048, 2048], P('fs', 'tp')
- key_moment_next: float32 [2048, 512], P('fs', 'tp')
- query_stat_next: float32 [32, 64, 64], P('tp')
- key_stat_next: float32 [8, 64, 64], P('tp')
Inputs may be any that keep to these rules, and one draw needn't show every extreme that they name: `query_row_root`: symmetric. `key_row_root`: symmetric. `query_head_root`: each head's matrix is symmetric. `key_head_root`: each head's matrix is symmetric. `query_head_stat`: each head's matrix is symmetric. `key_head_stat`: each head's matrix is symmetric.
All inputs are finite; a program needn't handle non-finite values.
Results may differ from a plain program's by a relative error of at most 0.0018.
The roundings to bfloat16 on the way count: a program that leaves them out, or rounds other values in their place, can miss the bound.
Values may be sent and summed in bfloat16 or wider, within the bound.
A program may use at most 128 MiB of HBM per device.

v0:
```python
import jax
import jax.numpy as jnp
from jax import lax
from jax.sharding import PartitionSpec as P

D = 2048
HEAD_DIM = 64


MOMENT_DECAY = 0.8
STAT_DECAY = 0.5
LEARN_RATE = 0.1
EPSILON = 1e-06


def head_gram(rounded, head_count):
    shaped = rounded.reshape(rounded.shape[0], head_count, HEAD_DIM)
    return jnp.einsum("rhd,rhe->hde", shaped, shaped, preferred_element_type=jnp.float32)


def column_factor(rounded, head_root):
    head_count = head_root.shape[0]
    shaped = rounded.reshape(rounded.shape[0], head_count, HEAD_DIM)
    rightward = jnp.einsum("rhd,hde->rhe", shaped, head_root, preferred_element_type=jnp.float32)
    return rightward.reshape(rounded.shape[0], head_count * HEAD_DIM).astype(jnp.bfloat16)


def shards(
    saved_input,
    query_cotangent,
    key_cotangent,
    query_weight,
    key_weight,
    query_moment,
    key_moment,
    query_row_root,
    key_row_root,
    query_head_root,
    key_head_root,
    query_head_stat,
    key_head_stat,
):
    query_width = query_cotangent.shape[1]
    cotangents = jnp.concatenate([query_cotangent, key_cotangent], axis=1)
    partial_value = lax.psum_scatter(
        lax.dot_general(
            saved_input, cotangents, (((0,), (0,)), ((), ())), preferred_element_type=jnp.float32
        ),
        ("fs", "rep"),
        scatter_dimension=0,
        tiled=True,
    )
    gradient = lax.all_gather(partial_value, "rep", axis=0, tiled=True)
    rounded = gradient.astype(jnp.bfloat16)
    query_rounded = rounded[:, :query_width]
    key_rounded = rounded[:, query_width:]
    query_gram, key_gram = lax.psum(
        (
            head_gram(query_rounded, query_head_root.shape[0]),
            head_gram(key_rounded, key_head_root.shape[0]),
        ),
        "fs",
    )
    query_stat_next = STAT_DECAY * query_head_stat + (1.0 - STAT_DECAY) * query_gram / D
    key_stat_next = STAT_DECAY * key_head_stat + (1.0 - STAT_DECAY) * key_gram / D
    query_right = column_factor(query_rounded, query_head_root)
    key_right = column_factor(key_rounded, key_head_root)
    query_piece = lax.all_gather(query_right, "fs", axis=0, tiled=True)
    key_piece = lax.all_gather(key_right, "fs", axis=0, tiled=True)
    query_pre = jnp.dot(query_row_root, query_piece, preferred_element_type=jnp.float32)
    key_pre = jnp.dot(key_row_root, key_piece, preferred_element_type=jnp.float32)
    query_moment_next = MOMENT_DECAY * query_moment + (1.0 - MOMENT_DECAY) * query_pre
    key_moment_next = MOMENT_DECAY * key_moment + (1.0 - MOMENT_DECAY) * key_pre
    query_wsq, query_msq, key_wsq, key_msq = lax.psum(
        (
            jnp.sum(query_weight * query_weight),
            jnp.sum(query_moment_next * query_moment_next),
            jnp.sum(key_weight * key_weight),
            jnp.sum(key_moment_next * key_moment_next),
        ),
        ("fs", "tp"),
    )
    query_step = (
        LEARN_RATE * (jnp.sqrt(query_wsq) / jnp.sqrt(query_msq + EPSILON)) * query_moment_next
    )
    key_step = LEARN_RATE * (jnp.sqrt(key_wsq) / jnp.sqrt(key_msq + EPSILON)) * key_moment_next
    query_next = query_weight - query_step
    key_next = key_weight - key_step
    query_copy, key_copy = (
        lax.all_gather(query_next.astype(jnp.bfloat16), "fs", axis=0, tiled=True),
        lax.all_gather(key_next.astype(jnp.bfloat16), "fs", axis=0, tiled=True),
    )
    return (
        query_step,
        key_step,
        query_next,
        key_next,
        query_copy,
        key_copy,
        query_moment_next,
        key_moment_next,
        query_stat_next,
        key_stat_next,
    )


def solution(mesh):
    in_specs = (
        P(("fs", "rep"), None),
        P(("fs", "rep"), "tp"),
        P(("fs", "rep"), "tp"),
        P("fs", "tp"),
        P("fs", "tp"),
        P("fs", "tp"),
        P("fs", "tp"),
        P("fs", None),
        P("fs", None),
        P("tp", None, None),
        P("tp", None, None),
        P("tp", None, None),
        P("tp", None, None),
    )
    out_specs = (
        P("fs", "tp"),
        P("fs", "tp"),
        P("fs", "tp"),
        P("fs", "tp"),
        P(None, "tp"),
        P(None, "tp"),
        P("fs", "tp"),
        P("fs", "tp"),
        P("tp", None, None),
        P("tp", None, None),
    )
    return jax.shard_map(shards, mesh=mesh, in_specs=in_specs, out_specs=out_specs, check_vma=False)
```

profile of v0, /device:TPU:0, one launch (start us, length us, event | category | flops | bytes accessed | tf_op | source)
XLA Modules:
  0.0 567.2 jit_solution(7115571609931742830)
XLA Ops:
  7.2 0.0 reduce-scatter.2.cloned.1.call-start
  7.2 10.8 %convolution_bitcast_fusion = f32[2048,1280]{0,1:T(8,128)} fusion(bf16[1024,2048]{1,0:T(8,128)(2,1)} %param.13, bf16[1024,256]{1,0:T(8,128)(2,1)} %param.15, bf16[1024,1024]{1,0:T(8,128)(2,1)} %param.14), kind=kOutput, calls=%fused_computation | convolution fusion | flops 5373952000 | bytes 17301504 | tf_op jit(solution)/shard_map/dot_general | solution.py:46
  18.0 0.0 reduce-scatter.2.cloned.1.call-update
  18.0 0.0 all-gather.6.cloned.1.call-start
  18.1 222.6 %reduce-scatter.2.cloned.1.call-done = f32[128,1280]{0,1:T(8,128)} async-done(((f32[2048,1280]{0,1:T(8,128)}), f32[128,1280]{0,1:T(8,128)}) %reduce-scatter.2.cloned.1.call-update) | async-done | bytes 655376 | tf_op jit(solution)/shard_map/reduce_scatter | solution.py:45
  240.7 0.0 all-gather.6.cloned.1.call-update
  240.7 0.0 all-gather.10.cloned.1.call-start
  240.8 44.8 %all-gather.6.cloned.1.call-done = f32[512,1280]{0,1:T(8,128)} async-done(((f32[128,1280]{0,1:T(8,128)}), f32[512,1280]{0,1:T(8,128)}) %all-gather.6.cloned.1.call-update) | async-done | bytes 2621456 | tf_op jit(solution)/shard_map/all_gather | solution.py:53
  285.6 1.9 convert_element_type.27
  287.5 1.0 copy-done.4
  288.6 1.0 convolution_convert_fusion.1
  289.5 0.0 all-gather.10.cloned.1.call-update
  289.6 0.0 all-gather.8.cloned.1.call-start
  289.6 1.3 slice.8
  290.9 2.4 convolution_convert_fusion
  293.3 0.0 all-gather.8.cloned.1.call-update
  293.3 0.0 all-reduce.4.cloned.1.call-start
  293.4 2.9 copy.23
  296.3 2.1 copy.25
  298.3 2.0 copy.28
  300.4 1.8 multiply_reduce_fusion.3
  302.2 2.7 multiply_reduce_fusion.1
  304.9 0.9 fusion.9
  305.8 1.2 fusion.8
  307.0 0.0 all-gather.14.cloned.1.call-start
  307.0 10.7 %all-gather.10.cloned.1.call-done = bf16[2048,256]{0,1:T(8,128)(2,1)} async-done(((bf16[512,256]{0,1:T(8,128)(2,1)}), bf16[2048,256]{0,1:T(8,128)(2,1)}) %all-gather.10.cloned.1.call-update) | async-done | bytes 1048592 | tf_op jit(solution)/shard_map/all_gather | solution.py:69
  317.7 3.4 multiply_reduce_fusion.2
  321.1 78.7 %all-gather.8.cloned.1.call-done = bf16[2048,1024]{0,1:T(8,128)(2,1)} async-done(((bf16[512,1024]{0,1:T(8,128)(2,1)}), bf16[2048,1024]{0,1:T(8,128)(2,1)}) %all-gather.8.cloned.1.call-update) | async-done | bytes 4194320 | tf_op jit(solution)/shard_map/all_gather | solution.py:68
  399.8 7.2 %multiply_reduce_fusion = (f32[]{:T(128)}, f32[512,1024]{0,1:T(8,128)}) fusion(bf16[2048,1024]{0,1:T(8,128)(2,1)} %all-gather.8.cloned.1.call-done, bf16[512,2048]{1,0:T(8,128)(2,1)S(1)} %copy-done, f32[512,1024]{0,1:T(8,128)} %copy.23), kind=kOutput, calls=%fused_computation.5 | convolution fusion | flops 2150105088 | bytes 10485764 | tf_op jit(solution)/shard_map/dot_general | solution.py:70
  407.1 14.9 %all-reduce = (f32[]{:T(128)}, f32[]{:T(128)}, f32[]{:T(128)}, f32[]{:T(128)}) all-reduce(f32[]{:T(128)} %multiply_reduce_fusion.1, f32[]{:T(128)} %get-tuple-element.32, f32[]{:T(128)} %multiply_reduce_fusion.3, f32[]{:T(128)} %get-tuple-element.34), channel_id=1, replica_groups=mesh['fs'=4,'rep'=4,'tp'=2] {'fs','tp'}, use_global_device_ids=true, to_apply=%region_1.0 | all-reduce | flops 4 | bytes 32 | tf_op jit(solution)/shard_map/psum | solution.py:74
  423.4 2.1 fusion.6
  425.4 0.0 all-gather.14.cloned.1.call-update
  425.5 0.0 all-gather.12.cloned.1.call-start
  425.5 3.0 copy.27
  429.9 4.7 fusion.7
  434.6 8.0 %all-reduce.4.cloned.1.call-done = (f32[16,64,64]{2,1,0:T(8,128)}, f32[4,64,64]{2,1,0:T(8,128)}) async-done(((f32[16,64,64]{2,1,0:T(8,128)}, f32[4,64,64]{2,1,0:T(8,128)}), (f32[16,64,64]{2,1,0:T(8,128)}, f32[4,64,64]{2,1,0:T(8,128)})) %all-reduce.4.cloned.1.call-update) | async-done | bytes 327696 | tf_op jit(solution)/shard_map/psum | solution.py:57
  442.6 1.6 multiply_add_fusion.1
  444.2 2.1 multiply_add_fusion
  446.3 1.0 copy.36
  447.3 1.8 copy.35
  449.1 3.0 copy.29
  452.1 1.0 copy.30
  453.1 1.8 copy.31
  454.9 1.0 copy.32
  455.9 16.1 %all-gather.14.cloned.1.call-done = bf16[2048,256]{0,1:T(8,128)(2,1)} async-done(((bf16[512,256]{0,1:T(8,128)(2,1)}), bf16[2048,256]{0,1:T(8,128)(2,1)}) %all-gather.14.cloned.1.call-update) | async-done | bytes 1048592 | tf_op jit(solution)/shard_map/all_gather | solution.py:91
  472.1 2.3 copy.34
  474.3 79.5 %all-gather.12.cloned.1.call-done = bf16[2048,1024]{0,1:T(8,128)(2,1)} async-done(((bf16[512,1024]{0,1:T(8,128)(2,1)}), bf16[2048,1024]{0,1:T(8,128)(2,1)}) %all-gather.12.cloned.1.call-update) | async-done | bytes 4194320 | tf_op jit(solution)/shard_map/all_gather | solution.py:90
  553.8 6.5 %copy.33 = bf16[2048,1024]{1,0:T(8,128)(2,1)} copy(bf16[2048,1024]{0,1:T(8,128)(2,1)} %all-gather.12.cloned.1.call-done) | data formatting | bytes 8388608
  (18 shorter events, 0.1 us)
Async XLA Ops:
  7.2 392.7 %copy-start = (bf16[512,2048]{1,0:T(8,128)(2,1)S(1)}, bf16[512,2048]{1,0:T(8,128)(2,1)}, u32[]{:S(2)}) copy-start(bf16[512,2048]{1,0:T(8,128)(2,1)} %param.20) | copy-start | bytes 6291460
  7.2 233.5 %reduce-scatter.2.cloned.1.call-start = ((), (), s32[]{:S(2)}) async-start(), calls=%async_computation.1 | async-start | bytes 11141120 | tf_op jit(solution)/shard_map/reduce_scatter | solution.py:45
  18.0 267.5 %all-gather.6.cloned.1.call-start = ((), (), s32[]{:S(2)}) async-start(), calls=%async_computation.2 | async-start | bytes 3276800 | tf_op jit(solution)/shard_map/all_gather | solution.py:53
  240.7 47.8 %copy-start.7 = (bf16[4,64,64]{2,1,0:T(8,128)(2,1)S(1)}, bf16[4,64,64]{2,1,0:T(8,128)(2,1)}, u32[]{:S(2)}) copy-start(bf16[4,64,64]{2,1,0:T(8,128)(2,1)} %param.23) | copy-start | bytes 98308
  240.7 77.0 %all-gather.10.cloned.1.call-start = ((), (), s32[]{:S(2)}) async-start(), calls=%async_computation.4 | async-start | bytes 1310720 | tf_op jit(solution)/shard_map/all_gather | solution.py:69
  287.5 1.1 copy-start.4
  289.6 110.3 %all-gather.8.cloned.1.call-start = ((), (), s32[]{:S(2)}) async-start(), calls=%async_computation.3 | async-start | bytes 5242880 | tf_op jit(solution)/shard_map/all_gather | solution.py:68
  293.3 149.3 %all-reduce.4.cloned.1.call-start = ((), (), s32[]{:S(2)}) async-start(), calls=%async_computation.7 | async-start | bytes 1310720 | tf_op jit(solution)/shard_map/psum | solution.py:57
  307.0 165.1 %all-gather.14.cloned.1.call-start = ((), (), s32[]{:S(2)}) async-start(), calls=%async_computation.6 | async-start | bytes 1310720 | tf_op jit(solution)/shard_map/all_gather | solution.py:91
  425.4 4.5 copy-start.2
  425.5 128.3 %all-gather.12.cloned.1.call-start = ((), (), s32[]{:S(2)}) async-start(), calls=%async_computation.5 | async-start | bytes 5242880 | tf_op jit(solution)/shard_map/all_gather | solution.py:90
  429.9 12.7 %copy-start.6 = (f32[4,64,64]{2,1,0:T(8,128)S(1)}, f32[4,64,64]{2,1,0:T(8,128)}, u32[]{:S(2)}) copy-start(f32[4,64,64]{2,1,0:T(8,128)} %param.25) | copy-start | bytes 196612
  449.1 3.0 copy-start.5
  449.1 4.0 copy-start.3
  553.8 6.5 %copy-start.1 = (bf16[512,2048]{1,0:T(8,128)(2,1)S(1)}, bf16[512,2048]{1,0:T(8,128)(2,1)}, u32[]{:S(2)}) copy-start(bf16[512,2048]{1,0:T(8,128)(2,1)} %param.20) | copy-start | bytes 6291460
Sparse Core Ops, SparseCore 0:
  18.1 222.5 reduce-scatter.1
  242.5 42.9 all-gather.5
  289.7 27.9 all-gather.9
  319.7 80.1 all-gather.7
  403.3 39.3 all-reduce.3
  444.6 27.3 all-gather.13
  473.6 80.1 all-gather.11
where the time goes:
time: 568 us; the launch traced here: 567 us
  waiting for transfers between devices  460 us (81%)
  local copies, waits for them, and re-layouts  30.8 us (5%)
  matrix products  26.8 us (5%)
  between operations  17 us (3%)
  other arithmetic  16.8 us (3%)
  blocking collectives  14.9 us (3%)
    reduce_scatter x1, waiting for transfers between devices, shards(): lax.psum_scatter(lax.dot_general(saved_input, cotangents, (((0,), (0,)),...  223 us
    all_gather x1, waiting for transfers between devices, shards(): lax.all_gather(query_next.astype(jnp.bfloat16), 'fs', axis=0, tiled=True)  79.5 us
    all_gather x1, waiting for transfers between devices, shards(): query_piece = lax.all_gather(query_right, 'fs', axis=0, tiled=True)  78.7 us
    all_gather x1, waiting for transfers between devices, shards(): gradient = lax.all_gather(partial_value, 'rep', axis=0, tiled=True)  44.8 us
    unnamed x28, local copies, waits for them, and re-layouts  29.5 us
    all_gather x1, waiting for transfers between devices, shards(): lax.all_gather(key_next.astype(jnp.bfloat16), 'fs', axis=0, tiled=True)  16.1 us
    psum x1, blocking collectives, shards(): lax.psum((jnp.sum(query_weight * query_weight), jnp.sum(query_moment_next...  14.9 us
  transfers between devices with their start and end apart: 7, of which 7 were waited for; matrix products, arithmetic and copies ran while one was open for 9% of the time, Pallas kernels for 0%

commit v1 on v0

v1 whole, which is shorter than its diff:
```python
import functools

import jax
import jax.numpy as jnp
from jax import lax
from jax.experimental import pallas as pl
from jax.experimental.pallas import tpu as pltpu
from jax.sharding import PartitionSpec as P

HEAD_DIM = 64
LANES = 128

MOMENT_DECAY = 0.8
STAT_DECAY = 0.5
LEARN_RATE = 0.1
EPSILON = 1e-06


def log2(n):
    return n.bit_length() - 1


class Cube:
    def __init__(self, fs, rep, block):
        self.fs, self.rep, self.block = fs, rep, block
        self.low, self.high = log2(rep), log2(fs)
        self.dims = self.low + self.high
        f, r = lax.axis_index("fs"), lax.axis_index("rep")
        self.f, self.r = f, r
        self.bits = [(r // 2**k) % 2 for k in range(self.low)]
        self.bits += [(f // 2**k) % 2 for k in range(self.high)]
        self.me = f * rep + r

    def partner(self, bit):
        flip = 1 - 2 * self.bits[bit]
        if bit < self.low:
            return {"rep": self.r + flip * 2**bit}
        return {"fs": self.f + flip * 2 ** (bit - self.low)}

    def rows(self, free, j, flipped=None):
        index = self.me
        for k, bit in enumerate(free):
            index = index + ((j // 2**k) % 2) * ((1 - 2 * self.bits[bit]) * 2**bit)
        if flipped is not None:
            index = index + (1 - 2 * self.bits[flipped]) * 2**flipped
        return pl.ds(pl.multiple_of(index * self.block, self.block), self.block)

    def barrier(self):
        barrier = pltpu.get_barrier_semaphore()
        for bit in range(self.dims):
            pl.semaphore_signal(
                barrier, inc=1, device_id=self.partner(bit), device_id_type=pl.DeviceIdType.MESH
            )
        pl.semaphore_wait(barrier, self.dims)


def each(start, stop, body):
    if stop - start <= 8:
        for j in range(start, stop):
            body(j)
    else:
        lax.fori_loop(start, stop, lambda j, _: (body(j), 0)[1], 0)


def orders(low, high):
    rep_bits, fs_bits = list(range(low)), list(range(low, low + high))
    near, far = fs_bits[:1], fs_bits[1:]
    return {
        "a": rep_bits + near + far,
        "b": rep_bits[::-1] + near + far,
        "c": near + rep_bits + far,
        "d": near + rep_bits[::-1] + far,
    }


KINDS = "abcababdab"


def drain(ref, sem):
    pltpu.make_async_copy(ref, ref, sem).wait()


def gather_sends(cube, held, chunk, order, step, send_sem, recv_sem, known_plane):
    bit = order[step]
    free = sorted(order[:step])
    start = 0
    if known_plane and bit < cube.low:
        start = 2 ** len([b for b in free if b < cube.low])

    def send(j):
        rows = cube.rows(free, j)
        pltpu.make_async_remote_copy(
            src_ref=held.at[chunk, rows],
            dst_ref=held.at[chunk, rows],
            send_sem=send_sem.at[chunk, step],
            recv_sem=recv_sem.at[chunk, step],
            device_id=cube.partner(bit),
            device_id_type=pl.DeviceIdType.MESH,
        ).start()

    each(start, 2**step, send)
    return (2**step - start) * cube.block


def reduce_kernel(
    fs, rep, kinds, partial_ref, root_ref, right_ref, gram_ref, acc, landed, held,
    load_sem, rs_send, rs_recv, ag_send, ag_recv,
):
    block = acc.shape[1] // (fs * rep)
    cube = Cube(fs, rep, block)
    chunks = len(kinds)
    dims = cube.dims
    table = orders(cube.low, cube.high)

    loads = []
    for c in range(chunks):
        load = pltpu.make_async_copy(
            partial_ref.at[:, pl.ds(c * LANES, LANES)], acc.at[c], load_sem.at[c]
        )
        load.start()
        loads.append(load)
    cube.barrier()

    offsets = []
    total = 0
    for s in range(dims):
        offsets.append(total)
        total += 2 ** (dims - 1 - s) * block

    def absorb(c, s):
        order = table[kinds[c]]
        count = 2 ** (dims - 1 - s)
        drain(landed.at[c, pl.ds(offsets[s], count * block)], rs_recv.at[c, s])
        free = order[s + 1:]

        def add(j):
            rows = cube.rows(free, j)
            got = landed[c, pl.ds(offsets[s] + j * block, block)]
            acc[c, rows] = acc[c, rows] + got

        each(0, count, add)

    def reduce_send(c, s):
        order = table[kinds[c]]
        bit = order[s]
        free = order[s + 1:]

        def send(j):
            pltpu.make_async_remote_copy(
                src_ref=acc.at[c, cube.rows(free, j, flipped=bit)],
                dst_ref=landed.at[c, pl.ds(offsets[s] + j * block, block)],
                send_sem=rs_send.at[c, s],
                recv_sem=rs_recv.at[c, s],
                device_id=cube.partner(bit),
                device_id_type=pl.DeviceIdType.MESH,
            ).start()

        each(0, 2 ** (dims - 1 - s), send)

    def finish(c):
        gathered = held[c]
        right = jnp.dot(gathered, root_ref[c], preferred_element_type=jnp.float32)
        right_ref[:, pl.ds(c * LANES, LANES)] = right.astype(jnp.bfloat16)
        gram_ref[c] = lax.dot_general(
            gathered, gathered, (((0,), (0,)), ((), ())), preferred_element_type=jnp.float32
        )

    def stage(c, s):
        if s == 0:
            loads[c].wait()
        elif s <= dims:
            absorb(c, s - 1)
        if s < dims:
            reduce_send(c, s)
            return
        order = table[kinds[c]][::-1]
        step = s - dims
        if step == 0:
            mine = cube.rows([], 0)
            held[c, mine] = acc[c, mine].astype(jnp.bfloat16)
        else:
            drain(held.at[c, pl.ds(0, 2 ** (step - 1) * block)], ag_recv.at[c, step - 1])
        if step < dims:
            gather_sends(cube, held, c, order, step, ag_send, ag_recv, False)
        else:
            finish(c)

    plan = []
    for c in range(chunks):
        late = 0 if c < 6 else 1
        rank = c if c < 3 else (c + 4 if c < 6 else c - 3)
        for s in range(2 * dims + 1):
            plan.append((s + late, rank, c, s))
    for _, _, c, s in sorted(plan):
        stage(c, s)

    for c in range(chunks):
        for s in range(dims):
            drain(acc.at[c, pl.ds(0, 2 ** (dims - 1 - s) * block)], rs_send.at[c, s])
            drain(held.at[c, pl.ds(0, 2**s * block)], ag_send.at[c, s])


def reduce_rows(partial_value, roots, fs, rep):
    height, width = partial_value.shape
    chunks = width // LANES
    kinds = (KINDS * chunks)[:chunks]
    dims = log2(fs * rep)
    block = height // (fs * rep)
    return pl.pallas_call(
        functools.partial(reduce_kernel, fs, rep, kinds),
        name="reduce_rows",
        out_shape=(
            jax.ShapeDtypeStruct((height, width), jnp.bfloat16),
            jax.ShapeDtypeStruct((chunks, LANES, LANES), jnp.float32),
        ),
        in_specs=[
            pl.BlockSpec(memory_space=pl.ANY),
            pl.BlockSpec(memory_space=pltpu.VMEM),
        ],
        out_specs=[pl.BlockSpec(memory_space=pltpu.VMEM)] * 2,
        scratch_shapes=[
            pltpu.VMEM((chunks, height, LANES), jnp.float32),
            pltpu.VMEM((chunks, height - block, LANES), jnp.float32),
            pltpu.VMEM((chunks, height, LANES), jnp.bfloat16),
            pltpu.SemaphoreType.DMA((chunks,)),
            pltpu.SemaphoreType.DMA((chunks, dims)),
            pltpu.SemaphoreType.DMA((chunks, dims)),
            pltpu.SemaphoreType.DMA((chunks, dims)),
            pltpu.SemaphoreType.DMA((chunks, dims)),
        ],
        compiler_params=pltpu.CompilerParams(
            collective_id=0, has_side_effects=True, vmem_limit_bytes=60 * 2**20
        ),
    )(partial_value, roots)


def copy_kernel(
    fs, rep, kinds, query_ref, key_ref, query_out, key_out, held, load_sem, store_sem, send_sem, recv_sem
):
    height = held.shape[1]
    block = height // (fs * rep)
    cube = Cube(fs, rep, block)
    chunks = len(kinds)
    dims = cube.dims
    table = orders(cube.low, cube.high)
    split = query_ref.shape[1] // LANES
    plane = pl.ds(pl.multiple_of(cube.f * (height // fs), height // fs), height // fs)

    def columns(c, query, key):
        ref, at = (query, c) if c < split else (key, c - split)
        return ref.at[:, pl.ds(at * LANES, LANES)]

    loads = []
    for c in range(chunks):
        load = pltpu.make_async_copy(
            columns(c, query_ref, key_ref), held.at[c, plane], load_sem.at[c]
        )
        load.start()
        loads.append(load)
    cube.barrier()

    sent = {}
    stores = []

    def stage(c, s):
        order = table[kinds[c]][::-1]
        if s == 0:
            loads[c].wait()
        else:
            drain(held.at[c, pl.ds(0, sent[c, s - 1])], recv_sem.at[c, s - 1])
        if s < dims:
            sent[c, s] = gather_sends(cube, held, c, order, s, send_sem, recv_sem, True)
        else:
            store = pltpu.make_async_copy(
                held.at[c], columns(c, query_out, key_out), store_sem.at[c]
            )
            store.start()
            stores.append(store)

    for s in range(dims + 1):
        for c in range(chunks):
            stage(c, s)
    for store in stores:
        store.wait()
    for (c, s), size in sent.items():
        drain(held.at[c, pl.ds(0, size)], send_sem.at[c, s])


def gather_copies(query, key, fs, rep):
    height = query.shape[0] * fs
    chunks = (query.shape[1] + key.shape[1]) // LANES
    kinds = (KINDS * chunks)[:chunks]
    dims = log2(fs * rep)
    return pl.pallas_call(
        functools.partial(copy_kernel, fs, rep, kinds),
        name="gather_copies",
        out_shape=(
            jax.ShapeDtypeStruct((height, query.shape[1]), jnp.bfloat16),
            jax.ShapeDtypeStruct((height, key.shape[1]), jnp.bfloat16),
        ),
        in_specs=[pl.BlockSpec(memory_space=pl.ANY)] * 2,
        out_specs=[pl.BlockSpec(memory_space=pl.ANY)] * 2,
        scratch_shapes=[
            pltpu.VMEM((chunks, height, LANES), jnp.bfloat16),
            pltpu.SemaphoreType.DMA((chunks,)),
            pltpu.SemaphoreType.DMA((chunks,)),
            pltpu.SemaphoreType.DMA((chunks, dims)),
            pltpu.SemaphoreType.DMA((chunks, dims)),
        ],
        compiler_params=pltpu.CompilerParams(
            collective_id=1, has_side_effects=True, vmem_limit_bytes=32 * 2**20
        ),
    )(query, key)


def pair_roots(query_head_root, key_head_root):
    roots = jnp.concatenate([query_head_root, key_head_root], axis=0)
    roots = roots.reshape(-1, 2, HEAD_DIM, HEAD_DIM)
    zero = jnp.zeros_like(roots[:, 0])
    upper = jnp.concatenate([roots[:, 0], zero], axis=2)
    lower = jnp.concatenate([zero, roots[:, 1]], axis=2)
    return jnp.concatenate([upper, lower], axis=1)


def unpair(grams):
    first = grams[:, :HEAD_DIM, :HEAD_DIM]
    second = grams[:, HEAD_DIM:, HEAD_DIM:]
    return jnp.stack([first, second], axis=1).reshape(-1, HEAD_DIM, HEAD_DIM)


def shards(
    fs,
    rep,
    saved_input,
    query_cotangent,
    key_cotangent,
    query_weight,
    key_weight,
    query_moment,
    key_moment,
    query_row_root,
    key_row_root,
    query_head_root,
    key_head_root,
    query_head_stat,
    key_head_stat,
):
    height = saved_input.shape[1]
    query_width = query_cotangent.shape[1]
    query_heads = query_head_root.shape[0]
    cotangents = jnp.concatenate([query_cotangent, key_cotangent], axis=1)
    partial_value = lax.dot_general(
        saved_input, cotangents, (((0,), (0,)), ((), ())), preferred_element_type=jnp.float32
    )
    right, grams = reduce_rows(partial_value, pair_roots(query_head_root, key_head_root), fs, rep)
    grams = unpair(grams)
    query_stat_next = (
        STAT_DECAY * query_head_stat + (1.0 - STAT_DECAY) * grams[:query_heads] / height
    )
    key_stat_next = STAT_DECAY * key_head_stat + (1.0 - STAT_DECAY) * grams[query_heads:] / height
    query_pre = jnp.dot(
        query_row_root, right[:, :query_width], preferred_element_type=jnp.float32
    )
    key_pre = jnp.dot(key_row_root, right[:, query_width:], preferred_element_type=jnp.float32)
    query_moment_next = MOMENT_DECAY * query_moment + (1.0 - MOMENT_DECAY) * query_pre
    key_moment_next = MOMENT_DECAY * key_moment + (1.0 - MOMENT_DECAY) * key_pre
    query_wsq, query_msq, key_wsq, key_msq = lax.psum(
        (
            jnp.sum(query_weight * query_weight),
            jnp.sum(query_moment_next * query_moment_next),
            jnp.sum(key_weight * key_weight),
            jnp.sum(key_moment_next * key_moment_next),
        ),
        ("fs", "tp"),
    )
    query_step = (
        LEARN_RATE * (jnp.sqrt(query_wsq) / jnp.sqrt(query_msq + EPSILON)) * query_moment_next
    )
    key_step = LEARN_RATE * (jnp.sqrt(key_wsq) / jnp.sqrt(key_msq + EPSILON)) * key_moment_next
    query_next = query_weight - query_step
    key_next = key_weight - key_step
    query_copy, key_copy = gather_copies(
        query_next.astype(jnp.bfloat16), key_next.astype(jnp.bfloat16), fs, rep
    )
    return (
        query_step,
        key_step,
        query_next,
        key_next,
        query_copy,
        key_copy,
        query_moment_next,
        key_moment_next,
        query_stat_next,
        key_stat_next,
    )


def solution(mesh):
    in_specs = (
        P(("fs", "rep"), None),
        P(("fs", "rep"), "tp"),
        P(("fs", "rep"), "tp"),
        P("fs", "tp"),
        P("fs", "tp"),
        P("fs", "tp"),
        P("fs", "tp"),
        P("fs", None),
        P("fs", None),
        P("tp", None, None),
        P("tp", None, None),
        P("tp", None, None),
        P("tp", None, None),
    )
    out_specs = (
        P("fs", "tp"),
        P("fs", "tp"),
        P("fs", "tp"),
        P("fs", "tp"),
        P(None, "tp"),
        P(None, "tp"),
        P("fs", "tp"),
        P("fs", "tp"),
        P("tp", None, None),
        P("tp", None, None),
    )
    body = functools.partial(shards, mesh.shape["fs"], mesh.shape["rep"])
    return jax.shard_map(body, mesh=mesh, in_specs=in_specs, out_specs=out_specs, check_vma=False)
```

time: 568 us -> 259 us (0.46)
  waiting for transfers between devices: 460 us -> 0 us
  Pallas kernels: 0 us -> 205 us
  local copies, waits for them, and re-layouts: 30.8 us -> 5.93 us
  between operations: 17 us -> 3.57 us
  matrix products: 26.8 us -> 17.5 us
    all_gather x5 -> x0, waiting for transfers between devices: 230 us -> none  [the longest x1 79.5 us: shards(): lax.all_gather(query_next.astype(jnp.bfloat16), 'fs', axis=0, tiled=True)]
    reduce_scatter x1 -> x0, waiting for transfers between devices: 223 us -> none  [shards(): lax.psum_scatter(lax.dot_general(saved_input, cotangents, (((0,), (0,)),...]
    pallas_call x0 -> x2, Pallas kernels: none -> 205 us  [the longest x1 159 us: reduce_rows(): pl.pallas_call(functools.partial(reduce_kernel, fs, rep, kinds), name='re...]
    unnamed x28 -> x26, local copies, waits for them, and re-layouts: 29.5 us -> 4.47 us
    dot_general x6 -> x2, matrix products: 16.1 us -> 7.4 us  [the longest x1 4.33 us: shards(): jnp.dot(query_row_root, right[:, :query_width], preferred_element_type=jn...]
    psum x1 -> x0, waiting for transfers between devices: 7.98 us -> none  [shards(): lax.psum((head_gram(query_rounded, query_head_root.shape[0]), head_gram(k...]
  transfers between devices with their start and end apart: 7 -> 0, of which waited for: 7 -> 0; matrix products, arithmetic and copies ran while one was open for 9% -> 0% of each run, Pallas kernels for 0% -> 0%
where the time goes in v1:
time: 259 us
  Pallas kernels  205 us (79%)
  matrix products  17.5 us (7%)
  blocking collectives  14.2 us (5%)
  other arithmetic  12.9 us (5%)
  local copies, waits for them, and re-layouts  5.93 us (2%)
  between operations  3.57 us (1%)
    pallas_call x1, Pallas kernels, reduce_rows(): pl.pallas_call(functools.partial(reduce_kernel, fs, rep, kinds), name='re...  159 us
    pallas_call x1, Pallas kernels, gather_copies(): pl.pallas_call(functools.partial(copy_kernel, fs, rep, kinds), name='gath...  45.8 us
    psum x1, blocking collectives, shards(): lax.psum((jnp.sum(query_weight * query_weight), jnp.sum(query_moment_next...  14.2 us
    dot_general x1, matrix products, shards(): lax.dot_general(saved_input, cotangents, (((0,), (0,)), ((), ())), prefer...  10.1 us

profile of v1, /device:TPU:0, one launch (start us, length us, event | category | flops | bytes accessed | tf_op | source)
XLA Modules:
  0.0 258.6 jit_solution(12224207920472317894)
XLA Ops:
  0.6 0.0 copy-start
  0.7 0.0 copy-start.7
  0.7 0.0 copy-start.5
  0.7 0.0 copy-start.9
  0.7 1.9 multiply_reduce_fusion.3
  2.6 2.8 %multiply_reduce_fusion.1 = f32[]{:T(128)} fusion(f32[512,1024]{1,0:T(8,128)} %param.16), kind=kLoop, calls=%fused_computation.8 | loop fusion | flops 1048575 | bytes 2097156 | tf_op jit(solution)/shard_map/reduce_sum | solution.py:369
  5.4 0.0 copy-done.7
  5.4 0.0 copy-done.5
  5.4 0.1 pad_maximum_fusion
  5.5 0.8 fusion.14.root_ref
  6.4 0.0 copy-done.9
  6.4 10.1 %convolution_bitcast_fusion.partial_ref = f32[2048,1280]{1,0:T(8,128)} fusion(bf16[1024,2048]{1,0:T(8,128)(2,1)S(1)} %copy-done.9, bf16[1024,256]{1,0:T(8,128)(2,1)} %param.15, bf16[1024,1024]{1,0:T(8,128)(2,1)} %param.14), kind=kOutput, calls=%fused_computation | convolution fusion | flops 5373952000 | bytes 17301504 | tf_op jit(solution)/shard_map/dot_general | solution.py:352
  16.4 158.7 %reduce_rows.1 = (bf16[2048,1280]{1,0:T(8,128)(2,1)}, f32[10,128,128]{2,1,0:T(8,128)}) custom-call(f32[2048,1280]{1,0:T(8,128)} %convolution_bitcast_fusion.partial_ref, bf16[10,128,128]{2,1,0:T(8,128)(2,1)} %fusion.14.root_ref), custom_call_target="tpu_custom_call" | custom-call | tf_op jit(solution)/shard_map/reduce_rows/pallas_call | solution.py:209
  175.1 0.0 copy-start.3
  175.2 0.0 copy-start.8
  175.2 1.4 slice_bitcast_fusion
  176.6 0.0 copy-start.6
  176.6 0.0 copy-start.11
  176.6 0.1 fusion.13
  176.7 0.0 copy-done.3
  176.7 0.9 bitcast_add_fusion.1
  177.6 0.5 copy-done.6
  178.1 0.7 bitcast_add_fusion.2
  178.8 0.0 copy-done.8
  178.8 0.0 copy-done.11
  178.8 0.0 copy-start.10
  178.8 3.1 %multiply_reduce_fusion.2 = (f32[]{:T(128)}, f32[512,256]{1,0:T(8,128)S(1)}) fusion(bf16[512,2048]{1,0:T(8,128)(2,1)} %param.21, bf16[2048,1280]{1,0:T(8,128)(2,1)S(1)} %copy-done.8, f32[512,256]{1,0:T(8,128)S(1)} %copy-done.11), kind=kOutput, calls=%fused_computation.23 | convolution fusion | flops 537526272 | bytes 4194308 | tf_op jit(solution)/shard_map/dot_general | solution.py:364
  181.9 0.0 copy-start.4
  181.9 0.0 copy-done
  181.9 0.0 copy-done.10
  181.9 0.0 copy-start.2
  181.9 4.3 %multiply_reduce_fusion = (f32[]{:T(128)}, f32[512,1024]{1,0:T(8,128)}) fusion(bf16[512,2048]{1,0:T(8,128)(2,1)S(1)} %copy-done, bf16[2048,1280]{1,0:T(8,128)(2,1)S(1)} %copy-done.8, f32[512,1024]{1,0:T(8,128)S(1)} %copy-done.10), kind=kOutput, calls=%fused_computation.7 | convolution fusion | flops 2150105088 | bytes 10485764 | tf_op jit(solution)/shard_map/dot_general | solution.py:361
  186.2 14.2 %all-reduce.2 = (f32[]{:T(128)}, f32[]{:T(128)}, f32[]{:T(128)}, f32[]{:T(128)}) all-reduce(f32[]{:T(128)} %multiply_reduce_fusion.1, f32[]{:T(128)} %get-tuple-element.32, f32[]{:T(128)} %multiply_reduce_fusion.3, f32[]{:T(128)} %get-tuple-element.34), channel_id=1, replica_groups=mesh['fs'=4,'rep'=4,'tp'=2] {'fs','tp'}, use_global_device_ids=true, to_apply=%region_1.0 | all-reduce | flops 4 | bytes 32 | tf_op jit(solution)/shard_map/psum | solution.py:367
  203.2 0.0 copy-done.4
  203.2 0.0 copy-done.2
  203.2 0.0 copy-start.1
  203.2 1.1 fusion.17
  204.3 0.9 copy-done.1
  205.2 4.6 %fusion.18 = (bf16[512,1024]{1,0:T(8,128)(2,1)S(1)}, f32[512,1024]{1,0:T(8,128)}, f32[512,1024]{1,0:T(8,128)}) fusion(f32[512,1024]{1,0:T(8,128)S(1)} %copy-done.1, f32[512,1024]{1,0:T(8,128)} %get-tuple-element.52, f32[]{:T(128)S(6)} %mul.75), kind=kLoop, calls=%fused_computation.37 | loop fusion | flops 1572864 | bytes 9437188 | tf_op jit(solution)/shard_map/convert_element_type | solution.py:383
  209.8 45.8 %gather_copies.1 = (bf16[2048,1024]{1,0:T(8,128)(2,1)S(1)}, bf16[2048,256]{1,0:T(8,128)(2,1)S(1)}) custom-call(bf16[512,1024]{1,0:T(8,128)(2,1)S(1)} %get-tuple-element.25.query_ref, bf16[512,256]{1,0:T(8,128)(2,1)S(1)} %get-tuple-element.22.key_ref), custom_call_target="tpu_custom_call" | custom-call | tf_op jit(solution)/shard_map/gather_copies/pallas_call | solution.py:294
  255.6 2.0 copy.40
  257.6 1.0 copy.41
  (4 shorter events, 0.1 us)
Async XLA Ops:
  0.6 181.2 %copy-start = (bf16[512,2048]{1,0:T(8,128)(2,1)S(1)}, bf16[512,2048]{1,0:T(8,128)(2,1)}, u32[]{:S(2)}) copy-start(bf16[512,2048]{1,0:T(8,128)(2,1)} %param.20) | copy-start | bytes 6291460
  0.7 4.8 %copy-start.7 = (bf16[4,64,64]{2,1,0:T(8,128)(2,1)S(1)}, bf16[4,64,64]{2,1,0:T(8,128)(2,1)}, u32[]{:S(2)}) copy-start(bf16[4,64,64]{2,1,0:T(8,128)(2,1)} %param.23) | copy-start | bytes 98308
  0.7 4.8 %copy-start.5 = (bf16[16,64,64]{2,1,0:T(8,128)(2,1)S(1)}, bf16[16,64,64]{2,1,0:T(8,128)(2,1)}, u32[]{:S(2)}) copy-start(bf16[16,64,64]{2,1,0:T(8,128)(2,1)} %param.22) | copy-start | bytes 393220
  0.7 5.7 %copy-start.9 = (bf16[1024,2048]{1,0:T(8,128)(2,1)S(1)}, bf16[1024,2048]{1,0:T(8,128)(2,1)}, u32[]{:S(2)}) copy-start(bf16[1024,2048]{1,0:T(8,128)(2,1)} %param.13) | copy-start | bytes 12582916
  175.1 1.6 copy-start.3
  175.2 3.6 %copy-start.8 = (bf16[2048,1280]{1,0:T(8,128)(2,1)S(1)}, bf16[2048,1280]{1,0:T(8,128)(2,1)}, u32[]{:S(2)}) copy-start(bf16[2048,1280]{1,0:T(8,128)(2,1)} %get-tuple-element.14) | copy-start | bytes 15728644
  176.6 1.6 copy-start.6
  176.6 2.2 copy-start.11
  178.8 3.1 %copy-start.10 = (f32[512,1024]{1,0:T(8,128)S(1)}, f32[512,1024]{1,0:T(8,128)}, u32[]{:S(2)}) copy-start(f32[512,1024]{1,0:T(8,128)} %param.18) | copy-start | bytes 6291460
  181.9 21.3 %copy-start.4 = (f32[512,256]{1,0:T(8,128)}, f32[512,256]{1,0:T(8,128)S(1)}, u32[]{:S(2)}) copy-start(f32[512,256]{1,0:T(8,128)S(1)} %get-tuple-element.53) | copy-start | bytes 1572868
  181.9 21.3 %copy-start.2 = (f32[512,256]{1,0:T(8,128)S(1)}, f32[512,256]{1,0:T(8,128)}, u32[]{:S(2)}) copy-start(f32[512,256]{1,0:T(8,128)} %param.17) | copy-start | bytes 1572868
  203.2 2.0 copy-start.1

commit v2 on v1

--- a/solution.py
+++ b/solution.py
@@ -73,7 +73,17 @@
     }
 
 
-KINDS = "abcababdab"
+KINDS = "abcdababab"
+
+
+def wavefront(chunks, last):
+    plan = []
+    for c in range(chunks):
+        delay = 2 * min(2, (max(c - 1, 0) * 3) // max(chunks - 1, 1))
+        for s in range(last + 1):
+            turn = 0 if s == 0 else (2 if s == last else 1)
+            plan.append((s + delay, turn, c, s))
+    return [(c, s) for _, _, c, s in sorted(plan)]
 
 
 def drain(ref, sem):
@@ -185,13 +195,7 @@
         else:
             finish(c)
 
-    plan = []
-    for c in range(chunks):
-        late = 0 if c < 6 else 1
-        rank = c if c < 3 else (c + 4 if c < 6 else c - 3)
-        for s in range(2 * dims + 1):
-            plan.append((s + late, rank, c, s))
-    for _, _, c, s in sorted(plan):
+    for c, s in wavefront(chunks, 2 * dims):
         stage(c, s)
 
     for c in range(chunks):
@@ -277,9 +281,8 @@
             store.start()
             stores.append(store)
 
-    for s in range(dims + 1):
-        for c in range(chunks):
-            stage(c, s)
+    for c, s in wavefront(chunks, dims):
+        stage(c, s)
     for store in stores:
         store.wait()
     for (c, s), size in sent.items():

time: 259 us -> 266 us (1.027)
  Pallas kernels: 205 us -> 211 us
    pallas_call x1, Pallas kernels: 45.8 us -> 53.4 us  [gather_copies(): pl.pallas_call(functools.partial(copy_kernel, fs, rep, kinds), name='gath...]
where the time goes in v2:
time: 266 us; the launch traced here: 265 us
  Pallas kernels  211 us (79%)
  matrix products  17.5 us (7%)
  blocking collectives  14.2 us (5%)
  other arithmetic  12.9 us (5%)
  local copies, waits for them, and re-layouts  5.93 us (2%)
  between operations  3.57 us (1%)
    pallas_call x1, Pallas kernels, reduce_rows(): pl.pallas_call(functools.partial(reduce_kernel, fs, rep, kinds), name='re...  158 us
    pallas_call x1, Pallas kernels, gather_copies(): pl.pallas_call(functools.partial(copy_kernel, fs, rep, kinds), name='gath...  53.4 us
    psum x1, blocking collectives, shards(): lax.psum((jnp.sum(query_weight * query_weight), jnp.sum(query_moment_next...  14.2 us
    dot_general x1, matrix products, shards(): lax.dot_general(saved_input, cotangents, (((0,), (0,)), ((), ())), prefer...  10.1 us

profile of v2, /device:TPU:0, one launch (start us, length us, event | category | flops | bytes accessed | tf_op | source)
XLA Modules:
  0.0 265.3 jit_solution(5776508505726310219)
XLA Ops:
  0.6 0.0 copy-start
  0.7 0.0 copy-start.7
  0.7 0.0 copy-start.5
  0.7 0.0 copy-start.9
  0.7 1.9 multiply_reduce_fusion.3
  2.6 2.8 %multiply_reduce_fusion.1 = f32[]{:T(128)} fusion(f32[512,1024]{1,0:T(8,128)} %param.16), kind=kLoop, calls=%fused_computation.8 | loop fusion | flops 1048575 | bytes 2097156 | tf_op jit(solution)/shard_map/reduce_sum | solution.py:372
  5.4 0.0 copy-done.7
  5.4 0.0 copy-done.5
  5.4 0.1 pad_maximum_fusion
  5.5 0.8 fusion.14.root_ref
  6.4 0.0 copy-done.9
  6.4 10.1 %convolution_bitcast_fusion.partial_ref = f32[2048,1280]{1,0:T(8,128)} fusion(bf16[1024,2048]{1,0:T(8,128)(2,1)S(1)} %copy-done.9, bf16[1024,256]{1,0:T(8,128)(2,1)} %param.15, bf16[1024,1024]{1,0:T(8,128)(2,1)} %param.14), kind=kOutput, calls=%fused_computation | convolution fusion | flops 5373952000 | bytes 17301504 | tf_op jit(solution)/shard_map/dot_general | solution.py:355
  16.4 157.8 %reduce_rows.1 = (bf16[2048,1280]{1,0:T(8,128)(2,1)}, f32[10,128,128]{2,1,0:T(8,128)}) custom-call(f32[2048,1280]{1,0:T(8,128)} %convolution_bitcast_fusion.partial_ref, bf16[10,128,128]{2,1,0:T(8,128)(2,1)} %fusion.14.root_ref), custom_call_target="tpu_custom_call" | custom-call | tf_op jit(solution)/shard_map/reduce_rows/pallas_call | solution.py:213
  174.2 0.0 copy-start.3
  174.2 0.0 copy-start.8
  174.2 1.4 slice_bitcast_fusion
  175.6 0.0 copy-start.6
  175.7 0.0 copy-start.11
  175.7 0.1 fusion.13
  175.8 0.0 copy-done.3
  175.8 0.9 bitcast_add_fusion.1
  176.7 0.5 copy-done.6
  177.2 0.7 bitcast_add_fusion.2
  177.9 0.0 copy-done.8
  177.9 0.0 copy-done.11
  177.9 0.0 copy-start.10
  177.9 3.1 %multiply_reduce_fusion.2 = (f32[]{:T(128)}, f32[512,256]{1,0:T(8,128)S(1)}) fusion(bf16[512,2048]{1,0:T(8,128)(2,1)} %param.21, bf16[2048,1280]{1,0:T(8,128)(2,1)S(1)} %copy-done.8, f32[512,256]{1,0:T(8,128)S(1)} %copy-done.11), kind=kOutput, calls=%fused_computation.23 | convolution fusion | flops 537526272 | bytes 4194308 | tf_op jit(solution)/shard_map/dot_general | solution.py:367
  180.9 0.0 copy-start.4
  180.9 0.0 copy-done
  181.0 0.0 copy-done.10
  181.0 0.0 copy-start.2
  181.0 4.3 %multiply_reduce_fusion = (f32[]{:T(128)}, f32[512,1024]{1,0:T(8,128)}) fusion(bf16[512,2048]{1,0:T(8,128)(2,1)S(1)} %copy-done, bf16[2048,1280]{1,0:T(8,128)(2,1)S(1)} %copy-done.8, f32[512,1024]{1,0:T(8,128)S(1)} %copy-done.10), kind=kOutput, calls=%fused_computation.7 | convolution fusion | flops 2150105088 | bytes 10485764 | tf_op jit(solution)/shard_map/dot_general | solution.py:364
  185.3 14.2 %all-reduce.2 = (f32[]{:T(128)}, f32[]{:T(128)}, f32[]{:T(128)}, f32[]{:T(128)}) all-reduce(f32[]{:T(128)} %multiply_reduce_fusion.1, f32[]{:T(128)} %get-tuple-element.32, f32[]{:T(128)} %multiply_reduce_fusion.3, f32[]{:T(128)} %get-tuple-element.34), channel_id=1, replica_groups=mesh['fs'=4,'rep'=4,'tp'=2] {'fs','tp'}, use_global_device_ids=true, to_apply=%region_1.0 | all-reduce | flops 4 | bytes 32 | tf_op jit(solution)/shard_map/psum | solution.py:370
  202.3 0.0 copy-done.4
  202.3 0.0 copy-done.2
  202.3 0.0 copy-start.1
  202.3 1.1 fusion.17
  203.4 0.9 copy-done.1
  204.3 4.6 %fusion.18 = (bf16[512,1024]{1,0:T(8,128)(2,1)S(1)}, f32[512,1024]{1,0:T(8,128)}, f32[512,1024]{1,0:T(8,128)}) fusion(f32[512,1024]{1,0:T(8,128)S(1)} %copy-done.1, f32[512,1024]{1,0:T(8,128)} %get-tuple-element.52, f32[]{:T(128)S(6)} %mul.75), kind=kLoop, calls=%fused_computation.37 | loop fusion | flops 1572864 | bytes 9437188 | tf_op jit(solution)/shard_map/convert_element_type | solution.py:386
  208.8 53.4 %gather_copies.1 = (bf16[2048,1024]{1,0:T(8,128)(2,1)S(1)}, bf16[2048,256]{1,0:T(8,128)(2,1)S(1)}) custom-call(bf16[512,1024]{1,0:T(8,128)(2,1)S(1)} %get-tuple-element.25.query_ref, bf16[512,256]{1,0:T(8,128)(2,1)S(1)} %get-tuple-element.22.key_ref), custom_call_target="tpu_custom_call" | custom-call | tf_op jit(solution)/shard_map/gather_copies/pallas_call | solution.py:297
  262.3 2.0 copy.40
  264.3 1.0 copy.41
  (4 shorter events, 0.1 us)
Async XLA Ops:
  0.6 180.3 %copy-start = (bf16[512,2048]{1,0:T(8,128)(2,1)S(1)}, bf16[512,2048]{1,0:T(8,128)(2,1)}, u32[]{:S(2)}) copy-start(bf16[512,2048]{1,0:T(8,128)(2,1)} %param.20) | copy-start | bytes 6291460
  0.7 4.8 %copy-start.7 = (bf16[4,64,64]{2,1,0:T(8,128)(2,1)S(1)}, bf16[4,64,64]{2,1,0:T(8,128)(2,1)}, u32[]{:S(2)}) copy-start(bf16[4,64,64]{2,1,0:T(8,128)(2,1)} %param.23) | copy-start | bytes 98308
  0.7 4.8 %copy-start.5 = (bf16[16,64,64]{2,1,0:T(8,128)(2,1)S(1)}, bf16[16,64,64]{2,1,0:T(8,128)(2,1)}, u32[]{:S(2)}) copy-start(bf16[16,64,64]{2,1,0:T(8,128)(2,1)} %param.22) | copy-start | bytes 393220
  0.7 5.7 %copy-start.9 = (bf16[1024,2048]{1,0:T(8,128)(2,1)S(1)}, bf16[1024,2048]{1,0:T(8,128)(2,1)}, u32[]{:S(2)}) copy-start(bf16[1024,2048]{1,0:T(8,128)(2,1)} %param.13) | copy-start | bytes 12582916
  174.2 1.6 copy-start.3
  174.2 3.6 %copy-start.8 = (bf16[2048,1280]{1,0:T(8,128)(2,1)S(1)}, bf16[2048,1280]{1,0:T(8,128)(2,1)}, u32[]{:S(2)}) copy-start(bf16[2048,1280]{1,0:T(8,128)(2,1)} %get-tuple-element.14) | copy-start | bytes 15728644
  175.6 1.6 copy-start.6
  175.7 2.2 copy-start.11
  177.9 3.1 %copy-start.10 = (f32[512,1024]{1,0:T(8,128)S(1)}, f32[512,1024]{1,0:T(8,128)}, u32[]{:S(2)}) copy-start(f32[512,1024]{1,0:T(8,128)} %param.18) | copy-start | bytes 6291460
  180.9 21.3 %copy-start.4 = (f32[512,256]{1,0:T(8,128)}, f32[512,256]{1,0:T(8,128)S(1)}, u32[]{:S(2)}) copy-start(f32[512,256]{1,0:T(8,128)S(1)} %get-tuple-element.53) | copy-start | bytes 1572868
  181.0 21.3 %copy-start.2 = (f32[512,256]{1,0:T(8,128)S(1)}, f32[512,256]{1,0:T(8,128)}, u32[]{:S(2)}) copy-start(f32[512,256]{1,0:T(8,128)} %param.17) | copy-start | bytes 1572868
  202.3 2.0 copy-start.1
